TPU v7x, 32 devices: a whole 2x2x4 slice. The times are simulated.
32 devices in a mesh: sp: 4 (over z), tp: 8 (over y, x, core).
Axes of the slice: x: 2, y: 2, z: 4, core: 2. Of those that a mesh axis runs over, the one named last changes fastest.
Arguments:
- tokens: bfloat16 [3072, 2048], P('sp'), may hold values from -6 to 6
- norm_gain: float32 [2048], replicated, may hold values from 0.5 to 80
- grid_query_weight: bfloat16 [2048, 2048], P(None, 'tp'), may hold values from -0.5 to 0.5
- grid_key_weight: bfloat16 [2048, 1024], P(None, 'tp'), may hold values from -0.5 to 0.5
- grid_value_weight: bfloat16 [2048, 1024], P(None, 'tp'), may hold values from -0.5 to 0.5
- grid_query_gain: float32 [128], replicated, may hold values from 1.6 to 6
- grid_key_gain: float32 [128], replicated, may hold values from 1.6 to 6
- local_query_weight: bfloat16 [2048, 2048], P(None, 'tp'), may hold values from -0.5 to 0.5
- local_key_weight: bfloat16 [2048, 1024], P(None, 'tp'), may hold values from -0.5 to 0.5
- local_value_weight: bfloat16 [2048, 1024], P(None, 'tp'), may hold values from -0.5 to 0.5
- sink_logit: float32 [16], P('tp'), may hold values from 1 to 6
- grid_out_weight: bfloat16 [2048, 2048], P('tp'), may hold values from -0.09375 to 0.09375
- local_out_weight: bfloat16 [2048, 2048], P('tp'), may hold values from -0.09375 to 0.09375
Outputs:
- mixed: bfloat16 [3072, 2048], P(('sp', 'tp'))
All inputs are finite; a program needn't handle non-finite values.
Results may differ from a plain program's by a relative error of at most 0.03.
Values may be sent and summed in bfloat16 or wider, within the bound.
No kernel may reach another device: no remote copies, remote signals or barrier semaphores. Data moves between devices by JAX's collectives and lax.ppermute only.
A program may use at most 192 MiB of HBM per device.

v0:
```python
import math

import jax
import jax.numpy as jnp
from jax import lax
from jax.sharding import PartitionSpec as P

HEAD = 128
WINDOW = 128
GRID_W = 64


EPSILON = 1e-06
ROPE_BASE = 10000.0


def padded(block, sides, width):
    for axis, dim in sides:
        count = lax.axis_size(axis)
        forward = [(i, i + 1) for i in range(count - 1)]
        backward = [(target, source) for source, target in forward]
        low = lax.ppermute(
            lax.slice_in_dim(block, block.shape[dim] - width, None, axis=dim), axis, forward
        )
        high = lax.ppermute(lax.slice_in_dim(block, 0, width, axis=dim), axis, backward)
        block = jnp.concatenate([low, block, high], axis=dim)
    return block


def rms_rows(values, gain):
    widened = values.astype(jnp.float32)
    return widened * lax.rsqrt(jnp.mean(widened * widened, axis=-1, keepdims=True) + EPSILON) * gain


def half_turn(part, angles):
    cosine = jnp.cos(angles)
    sine = jnp.sin(angles)
    cosine = jnp.concatenate([cosine, cosine], axis=-1)
    sine = jnp.concatenate([sine, sine], axis=-1)
    first, second = jnp.split(part, 2, axis=-1)
    turned = jnp.concatenate([-second, first], axis=-1)
    return part * cosine + turned * sine


def axial_turn(heads, positions):
    half_dim = heads.shape[-1] // 2
    inverse = ROPE_BASE ** (-jnp.arange(0, half_dim, 2, dtype=jnp.float32) / half_dim)
    row_angle = (positions // GRID_W).astype(jnp.float32)[:, None, None] * inverse
    col_angle = (positions % GRID_W).astype(jnp.float32)[:, None, None] * inverse
    return jnp.concatenate(
        [half_turn(heads[..., :half_dim], row_angle), half_turn(heads[..., half_dim:], col_angle)],
        axis=-1,
    )


def shards(
    tokens,
    norm_gain,
    grid_query_weight,
    grid_key_weight,
    grid_value_weight,
    grid_query_gain,
    grid_key_gain,
    local_query_weight,
    local_key_weight,
    local_value_weight,
    sink_logit,
    grid_out_weight,
    local_out_weight,
):
    row_count = tokens.shape[0]
    seq_devices = lax.axis_size("sp")
    total_rows = row_count * seq_devices
    offset = lax.axis_index("sp") * row_count
    positions = offset + jnp.arange(row_count, dtype=jnp.int32)
    normed = rms_rows(tokens, norm_gain).astype(jnp.bfloat16)
    score_scale = HEAD ** (-0.5)
    width = grid_out_weight.shape[1]

    def project(weight):
        return jnp.dot(normed, weight, preferred_element_type=jnp.float32).astype(jnp.bfloat16)

    grid_heads = grid_query_weight.shape[1] // HEAD
    grid_groups = grid_key_weight.shape[1] // HEAD
    group_size = grid_heads // grid_groups
    queries = (
        axial_turn(
            rms_rows(
                project(grid_query_weight).reshape(row_count, grid_heads, HEAD), grid_query_gain
            ),
            positions,
        )
        .astype(jnp.bfloat16)
        .reshape(row_count, grid_groups, group_size, HEAD)
    )
    keys = axial_turn(
        rms_rows(project(grid_key_weight).reshape(row_count, grid_groups, HEAD), grid_key_gain),
        positions,
    ).astype(jnp.bfloat16)
    values = project(grid_value_weight).reshape(row_count, grid_groups, HEAD)

    def absorb(carry, pieces):
        running, totals, summed = carry
        scores = (
            jnp.einsum("qhgd,shd->hgqs", queries, pieces[0], preferred_element_type=jnp.float32)
            * score_scale
        )
        highest = jnp.maximum(running, jnp.max(scores, axis=-1))
        factor = jnp.exp(running - highest)
        weights = jnp.exp(scores - highest[..., None])
        totals = totals * factor + jnp.sum(weights, axis=-1)
        summed = summed * factor[..., None] + jnp.einsum(
            "hgqs,shd->hgqd",
            weights.astype(jnp.bfloat16),
            pieces[1],
            preferred_element_type=jnp.float32,
        )
        return (highest, totals, summed)

    initial = (
        jnp.full((grid_groups, group_size, row_count), -jnp.inf, jnp.float32),
        jnp.zeros((grid_groups, group_size, row_count), jnp.float32),
        jnp.zeros((grid_groups, group_size, row_count, HEAD), jnp.float32),
    )
    all_keys, all_values = (
        lax.all_gather(keys, "sp", axis=0, tiled=True),
        lax.all_gather(values, "sp", axis=0, tiled=True),
    )
    shards_per_step = math.gcd(seq_devices, max(1, 2048 // row_count))
    step_rows = row_count * shards_per_step

    def visit(index, carry):
        start = index * step_rows
        piece_keys = lax.dynamic_slice_in_dim(all_keys, start, step_rows, 0)
        piece_values = lax.dynamic_slice_in_dim(all_values, start, step_rows, 0)
        return absorb(carry, (piece_keys, piece_values))

    state = lax.fori_loop(0, total_rows // step_rows, visit, initial)
    running, totals, summed = state
    grid_result = jnp.transpose(summed / totals[..., None], (2, 0, 1, 3))
    grid_result = grid_result.reshape(row_count, grid_heads * HEAD).astype(jnp.bfloat16)
    local_heads = local_query_weight.shape[1] // HEAD
    local_groups = local_key_weight.shape[1] // HEAD
    local_size = local_heads // local_groups
    blocks = row_count // WINDOW
    local_queries = project(local_query_weight).reshape(
        blocks, WINDOW, local_groups, local_size, HEAD
    )
    pairs = jnp.stack(
        [
            project(local_key_weight).reshape(row_count, local_groups, HEAD),
            project(local_value_weight).reshape(row_count, local_groups, HEAD),
        ],
        axis=1,
    )
    widened = padded(pairs, (("sp", 0),), WINDOW)
    framed = widened.reshape(blocks + 2, WINDOW, 2, local_groups, HEAD)
    band = jnp.concatenate([framed[:-2], framed[1:-1], framed[2:]], axis=1)
    scores = (
        jnp.einsum(
            "nqhgd,nshd->hgnqs", local_queries, band[:, :, 0], preferred_element_type=jnp.float32
        )
        * score_scale
    )
    relative = jnp.arange(3 * WINDOW)[None, :] - WINDOW - jnp.arange(WINDOW)[:, None]
    key_pos = (
        offset + jnp.arange(blocks)[:, None] * WINDOW - WINDOW + jnp.arange(3 * WINDOW)[None, :]
    )
    valid = (jnp.abs(relative) <= WINDOW)[None] & ((key_pos >= 0) & (key_pos < total_rows))[
        :, None, :
    ]
    scores = jnp.where(valid, scores, -jnp.inf)
    sink = sink_logit.reshape(local_groups, local_size, 1, 1, 1)
    top = jnp.maximum(jnp.max(scores, axis=-1, keepdims=True), sink)
    lifted = jnp.exp(scores - top)
    weights = (lifted / (jnp.sum(lifted, axis=-1, keepdims=True) + jnp.exp(sink - top))).astype(
        jnp.bfloat16
    )
    local_result = jnp.einsum(
        "hgnqs,nshd->nqhgd", weights, band[:, :, 1], preferred_element_type=jnp.float32
    )
    local_result = local_result.astype(jnp.bfloat16).reshape(row_count, local_heads * HEAD)
    joined = lax.psum_scatter(
        jnp.concatenate(
            [
                jnp.dot(grid_result, grid_out_weight, preferred_element_type=jnp.float32),
                jnp.dot(local_result, local_out_weight, preferred_element_type=jnp.float32),
            ],
            axis=1,
        ).astype(jnp.bfloat16),
        "tp",
        scatter_dimension=0,
        tiled=True,
    ).astype(jnp.float32)
    merged = joined[:, :width] + joined[:, width:]
    return merged.astype(jnp.bfloat16)


def solution(mesh):
    in_specs = (
        P("sp", None),
        P(),
        P(None, "tp"),
        P(None, "tp"),
        P(None, "tp"),
        P(),
        P(),
        P(None, "tp"),
        P(None, "tp"),
        P(None, "tp"),
        P("tp"),
        P("tp", None),
        P("tp", None),
    )
    out_specs = P(("sp", "tp"), None)
    return jax.shard_map(shards, mesh=mesh, in_specs=in_specs, out_specs=out_specs, check_vma=False)
```

profile of v0, /device:TPU:0, one launch (start us, length us, event | category | flops | bytes accessed | tf_op | source)
XLA Modules:
  0.0 194.1 jit_solution(18339366877715833661)
XLA Ops:
  6.5 2.7 %fusion.22 = f32[768]{0:T(1024)S(1)} fusion(bf16[768,2048]{1,0:T(8,128)(2,1)} %param.15), kind=kLoop, calls=%fused_computation.27 | loop fusion | flops 4717824 | bytes 3148800 | tf_op jit(solution)/shard_map/reduce_sum | solution.py:32
  9.5 0.8 fusion.24
  10.5 1.0 convolution_convert_fusion.5
  11.5 0.4 copy-done.31
  11.9 1.0 convolution_convert_fusion.6
  12.9 0.7 pad_maximum_fusion.11
  13.6 5.6 %collective-permute-start = (bf16[128,2,1,128]{3,0,2,1:T(8,128)(2,1)}, bf16[128,2,1,128]{3,0,2,1:T(8,128)(2,1)}, u32[]{:S(2)}, u32[]{:S(2)}) collective-permute-start(bf16[128,2,1,128]{3,0,2,1:T(8,128)(2,1)} %get-tuple-element.202), channel_id=1, source_target_pairs={{0,8},{8,16},{16,24},{1,9},{9,17},{17,25},{2,10},{10,18},{18,26},{... | collective-permute-start | bytes 196616 | tf_op jit(solution)/shard_map/ppermute | solution.py:22
  19.2 1.3 collective-permute-start.1
  20.6 1.4 multiply_sine_fusion.1
  22.0 0.7 sine_bitcast_fusion.1
  22.8 0.7 abs_compare_fusion
  23.5 4.0 %convolution_convert_fusion.3 = bf16[768,256]{1,0:T(8,128)(2,1)} fusion(bf16[768,2048]{1,0:T(8,128)(2,1)} %copy-done.4, bf16[2048,256]{1,0:T(8,128)(2,1)} %param.22), kind=kOutput, calls=%fused_computation.39 | convolution fusion | flops 805502976 | bytes 4587520 | tf_op jit(solution)/shard_map/dot_general | solution.py:81
  27.5 3.1 %multiply_reduce_fusion.1 = (f32[768]{0:T(1024)S(1)}, f32[768,128]{0,1:T(8,128)S(1)}) fusion(bf16[768,2048]{1,0:T(8,128)(2,1)} %copy-done.4, bf16[2048,128]{1,0:T(8,128)(2,1)S(1)} %copy-done.21), kind=kOutput, calls=%fused_computation.80 | convolution fusion | flops 403045632 | bytes 4066304 | tf_op jit(solution)/shard_map/dot_general | solution.py:81
  30.7 0.8 fusion.45
  31.6 21.4 %all_gather.6 = bf16[3072,1,128]{0,2,1:T(8,128)(2,1)} all-gather(bf16[768,1,128]{0,2,1:T(8,128)(2,1)S(1)} %pad_maximum_fusion.9), channel_id=1, replica_groups=mesh['sp'=4,'tp'=8] {'sp'}, dimensions={0}, use_global_device_ids=true | all-gather | bytes 983040 | tf_op jit(solution)/shard_map/all_gather | solution.py:126
  53.0 1.1 multiply_reduce_fusion
  54.3 0.3 multiply_multiply_fusion
  54.6 2.3 %slice_negate_fusion.1 = (f32[768,2,32]{2,0,1:T(8,128)}, f32[768,2,32]{2,0,1:T(8,128)}, f32[768,2,32]{2,0,1:T(8,128)}, f32[768,2,32]{2,0,1:T(8,128)}) fusion(f32[768,2,128]{2,0,1:T(8,128)S(1)} %multiply_multiply_fusion), kind=kLoop, calls=%fused_computation.56 | loop fusion | flops 98304 | bytes 1572864 | tf_op jit(solution)/shard_map/neg | solution.py:41
  56.9 0.9 copy.29
  57.8 0.9 copy.28
  58.7 0.9 copy.31
  59.7 0.9 copy.30
  60.6 3.1 %convolution_convert_fusion.7 = bf16[768,128]{1,0:T(8,128)(2,1)S(1)} fusion(bf16[768,2048]{1,0:T(8,128)(2,1)} %copy-done.4, bf16[2048,128]{1,0:T(8,128)(2,1)} %param.19), kind=kOutput, calls=%fused_computation.47 | convolution fusion | flops 402751488 | bytes 3866624 | tf_op jit(solution)/shard_map/dot_general | solution.py:81
  63.8 17.5 %all-gather = bf16[3072,128]{1,0:T(8,128)(2,1)S(1)} all-gather(bf16[768,128]{1,0:T(8,128)(2,1)S(1)} %convolution_convert_fusion.7), channel_id=2, replica_groups=mesh['sp'=4,'tp'=8] {'sp'}, dimensions={0}, use_global_device_ids=true | all-gather | bytes 983040 | tf_op jit(solution)/shard_map/all_gather | solution.py:127
  81.4 0.7 fusion.37
  82.3 29.1 %while.18 = (s32[]{:T(128)}, f32[1,2,768]{2,1,0:T(2,128)S(1)}, f32[1,2,768]{2,1,0:T(2,128)S(1)}, f32[1,2,768,128]{3,2,1,0:T(8,128)S(1)}, bf16[3072,1,128]{0,2,1:...) while((s32[]{:T(128)}, f32[1,2,768]{2,1,0:T(2,128)S(1)}, ...), condition=%wide.region_6.7_spmd.clone, body=%wide.region_3.6_spmd.clone.sunk | while | flops 1227432960 | bytes 68911312 | solution.py:138
  82.3 6.1 %bitcast_reduce_fusion.2 = (f32[2,768]{1,0:T(2,128)S(1)}, f32[1536,768,2]{1,0,2:T(8,128)}) fusion(bf16[768,1,2,128]{3,0,2,1:T(8,128)(2,1)S(1)} %get-tuple-element.300, bf16[3072,1,128]{0,2,1:T(8,128)(2,1)} %get-tuple-element.299, s32[]{:T(128)S(6)} %select_n.56), kind=kOutput, calls=%fused_computation.1.clone.1 | convolution fusion | flops 608696832 | bytes 10229764 | tf_op jit(solution)/shard_map/while/body/eval_jaxpr/qhgd,shd->hgqs/dot_general | solution.py:105
  88.4 5.4 %fusion.83 = f32[2,768]{1,0:T(2,128)S(1)} fusion(f32[1536,768,2]{1,0,2:T(8,128)} %get-tuple-element.271, f32[2,768]{1,0:T(2,128)S(1)} %bitcast.169), kind=kLoop, calls=%fused_computation.4.clone.1 | loop fusion | flops 7076352 | bytes 9449472 | tf_op jit(solution)/shard_map/while/body/eval_jaxpr/reduce_sum | solution.py:111
  93.8 0.9 copy-done.1
  94.8 2.1 %fusion.84 = f32[1,2,768,128]{3,2,1,0:T(8,128)S(1)} fusion(f32[1536,768,2]{1,0,2:T(8,128)S(1)} %copy-done.1, f32[2,768]{1,0:T(2,128)S(1)} %bitcast.170, f32[1,2,768,128]{3,2,1,0:T(8,128)S(1)} %get-tuple-element.287, bf16[3072,1,128]{2,0,1:T(8,128)(2,1)S(1)} %get-tuple-element.301, s32[]{:T(128)S(6)} %select_n.56, ...), kind=kOutput, calls=%fused_computation.8.clone.1 | convolution fusion | flops 611647488 | bytes 11415557 | tf_op jit(solution)/shard_map/while/body/eval_jaxpr/hgqs,shd->hgqd/dot_general | solution.py:112
  96.9 6.1 %bitcast_reduce_fusion.2 = (f32[2,768]{1,0:T(2,128)S(1)}, f32[1536,768,2]{1,0,2:T(8,128)}) fusion(bf16[768,1,2,128]{3,0,2,1:T(8,128)(2,1)S(1)} %get-tuple-element.300, bf16[3072,1,128]{0,2,1:T(8,128)(2,1)} %get-tuple-element.299, s32[]{:T(128)S(6)} %select_n.56), kind=kOutput, calls=%fused_computation.1.clone.1 | convolution fusion | flops 608696832 | bytes 10229764 | tf_op jit(solution)/shard_map/while/body/eval_jaxpr/qhgd,shd->hgqs/dot_general | solution.py:105
  103.0 5.4 %fusion.83 = f32[2,768]{1,0:T(2,128)S(1)} fusion(f32[1536,768,2]{1,0,2:T(8,128)} %get-tuple-element.271, f32[2,768]{1,0:T(2,128)S(1)} %bitcast.169), kind=kLoop, calls=%fused_computation.4.clone.1 | loop fusion | flops 7076352 | bytes 9449472 | tf_op jit(solution)/shard_map/while/body/eval_jaxpr/reduce_sum | solution.py:111
  108.4 0.9 copy-done.1
  109.3 2.1 %fusion.84 = f32[1,2,768,128]{3,2,1,0:T(8,128)S(1)} fusion(f32[1536,768,2]{1,0,2:T(8,128)S(1)} %copy-done.1, f32[2,768]{1,0:T(2,128)S(1)} %bitcast.170, f32[1,2,768,128]{3,2,1,0:T(8,128)S(1)} %get-tuple-element.287, bf16[3072,1,128]{2,0,1:T(8,128)(2,1)S(1)} %get-tuple-element.301, s32[]{:T(128)S(6)} %select_n.56, ...), kind=kOutput, calls=%fused_computation.8.clone.1 | convolution fusion | flops 611647488 | bytes 11415557 | tf_op jit(solution)/shard_map/while/body/eval_jaxpr/hgqs,shd->hgqd/dot_general | solution.py:112
  111.4 0.3 copy.33
  111.8 2.7 %convolution_convert_fusion.1 = bf16[768,2048]{1,0:T(8,128)(2,1)} fusion(bf16[768,256]{0,1:T(8,128)(2,1)S(1)} %bitcast.172, bf16[256,2048]{1,0:T(8,128)(2,1)S(1)} %copy-done), kind=kOutput, calls=%fused_computation.32 | convolution fusion | flops 806879232 | bytes 4587520 | tf_op jit(solution)/shard_map/dot_general | solution.py:186
  114.5 0.5 broadcast_and_fusion
  115.1 1.0 pad_maximum_fusion.4
  116.2 0.5 fusion.26
  116.8 0.6 fusion.25
  117.5 0.8 fusion.27
  118.3 0.4 copy.39
  118.8 1.0 convolution_convert_fusion
  119.8 0.9 copy-done.2
  120.7 3.4 %pad_maximum_fusion = bf16[768,4096]{1,0:T(8,128)(2,1)} fusion(bf16[768,2048]{1,0:T(8,128)(2,1)S(1)} %convolution_convert_fusion, bf16[768,2048]{1,0:T(8,128)(2,1)S(1)} %copy-done.2), kind=kLoop, calls=%fused_computation.30 | loop fusion | flops 12582912 | bytes 12582912 | tf_op jit(solution)/shard_map/concatenate | solution.py:184
  124.1 61.0 %reduce-scatter.2.cloned.1.call-done = bf16[96,4096]{1,0:T(8,128)(2,1)} async-done(((bf16[768,4096]{1,0:T(8,128)(2,1)}), bf16[96,4096]{1,0:T(8,128)(2,1)}) %reduce-scatter.2.cloned.1.call-update) | async-done | bytes 786448 | tf_op jit(solution)/shard_map/reduce_scatter | solution.py:183
  185.1 1.3 convert_element_type.122
  186.4 0.8 fusion.31
  (95 shorter events, 1.8 us)
Async XLA Ops:
  6.5 105.2 %copy-start = (bf16[256,2048]{1,0:T(8,128)(2,1)S(1)}, bf16[256,2048]{1,0:T(8,128)(2,1)}, u32[]{:S(2)}) copy-start(bf16[256,2048]{1,0:T(8,128)(2,1)} %param.26) | copy-start | bytes 3145732
  6.5 2.7 %copy-start.25 = (f32[2048]{0:T(1024)S(1)}, f32[2048]{0:T(1024)}, u32[]{:S(2)}) copy-start(f32[2048]{0:T(1024)} %param.16) | copy-start | bytes 24580
  6.5 178.6 %reduce-scatter.2.cloned.1.call-start = ((), (), s32[]{:S(2)}) async-start(), calls=%async_computation.1 | async-start | bytes 7077888 | tf_op jit(solution)/shard_map/reduce_scatter | solution.py:183
  6.5 2.9 %copy-start.3 = (bf16[768,2048]{1,0:T(8,128)(2,1)S(1)}, bf16[768,2048]{1,0:T(8,128)(2,1)}, u32[]{:S(2)}) copy-start(bf16[768,2048]{1,0:T(8,128)(2,1)} %param.15) | copy-start | bytes 9437188
  9.5 1.0 copy-start.30
  10.5 2.4 %copy-start.4 = (bf16[768,2048]{1,0:T(8,128)(2,1)}, bf16[768,2048]{1,0:T(8,128)(2,1)S(1)}, u32[]{:S(2)}) copy-start(bf16[768,2048]{1,0:T(8,128)(2,1)S(1)} %fusion.24) | copy-start | bytes 9437188
  10.5 1.4 copy-start.31
  11.9 1.0 copy-start.10
  12.9 0.7 copy-start.12
  13.6 101.5 %collective-permute-start = (bf16[128,2,1,128]{3,0,2,1:T(8,128)(2,1)}, bf16[128,2,1,128]{3,0,2,1:T(8,128)(2,1)}, u32[]{:S(2)}, u32[]{:S(2)}) collective-permute-start(bf16[128,2,1,128]{3,0,2,1:T(8,128)(2,1)} %get-tuple-element.202), channel_id=1, source_target_pairs={{0,8},{8,16},{16,24},{1,9},{9,17},{17,25},{2,10},{10,18},{18,26},{... | collective-permute-start | bytes 196616 | tf_op jit(solution)/shard_map/ppermute | solution.py:22
  19.2 95.9 %collective-permute-start.1 = (bf16[128,2,1,128]{3,0,2,1:T(8,128)(2,1)}, bf16[128,2,1,128]{3,0,2,1:T(8,128)(2,1)}, u32[]{:S(2)}, u32[]{:S(2)}) collective-permute-start(bf16[128,2,1,128]{3,0,2,1:T(8,128)(2,1)} %get-tuple-element.203), channel_id=1, source_target_pairs={{8,0},{16,8},{24,16},{9,1},{17,9},{25,17},{10,2},{18,10},{26,18},{... | collective-permute-start | bytes 196616 | tf_op jit(solution)/shard_map/ppermute | solution.py:25
  23.5 4.0 %copy-start.21 = (bf16[2048,128]{1,0:T(8,128)(2,1)S(1)}, bf16[2048,128]{1,0:T(8,128)(2,1)}, u32[]{:S(2)}) copy-start(bf16[2048,128]{1,0:T(8,128)(2,1)} %param.18) | copy-start | bytes 1572868
  27.5 3.1 %copy-start.28 = (f32[128]{0:T(128)S(1)}, f32[128]{0:T(128)}, u32[]{:S(2)}) copy-start(f32[128]{0:T(128)} %param.21) | copy-start | bytes 1540
  30.6 22.4 %copy-start.5 = (bf16[768,2048]{1,0:T(8,128)(2,1)S(1)}, bf16[768,2048]{1,0:T(8,128)(2,1)}, u32[]{:S(2)}) copy-start(bf16[768,2048]{1,0:T(8,128)(2,1)} %copy-done.4) | copy-start | bytes 9437188
  30.6 22.4 %copy-start.29 = (bf16[2048,256]{1,0:T(8,128)(2,1)S(1)}, bf16[2048,256]{1,0:T(8,128)(2,1)}, u32[]{:S(2)}) copy-start(bf16[2048,256]{1,0:T(8,128)(2,1)} %param.17) | copy-start | bytes 3145732
  53.0 1.3 copy-start.27
  54.5 2.3 %copy-start.23 = (f32[768,1,32]{0,2,1:T(8,128)S(1)}, f32[768,1,32]{0,2,1:T(8,128)}, u32[]{:S(2)}) copy-start(f32[768,1,32]{0,2,1:T(8,128)} %get-tuple-element.206) | copy-start | bytes 294916
  54.5 3.3 %copy-start.20 = (f32[768,64]{0,1:T(8,128)S(1)}, f32[768,64]{0,1:T(8,128)}, u32[]{:S(2)}) copy-start(f32[768,64]{0,1:T(8,128)} %get-tuple-element.205) | copy-start | bytes 589828
  54.6 5.1 %copy-start.19 = (f32[768,64]{0,1:T(8,128)S(1)}, f32[768,64]{0,1:T(8,128)}, u32[]{:S(2)}) copy-start(f32[768,64]{0,1:T(8,128)} %get-tuple-element.204) | copy-start | bytes 589828
  60.6 20.7 %copy-start.6 = (f32[768,2,32]{2,0,1:T(8,128)S(1)}, f32[768,2,32]{2,0,1:T(8,128)}, u32[]{:S(2)}) copy-start(f32[768,2,32]{2,0,1:T(8,128)} %get-tuple-element.190) | copy-start | bytes 589828
  60.6 20.7 %copy-start.7 = (f32[768,2,32]{2,0,1:T(8,128)S(1)}, f32[768,2,32]{2,0,1:T(8,128)}, u32[]{:S(2)}) copy-start(f32[768,2,32]{2,0,1:T(8,128)} %get-tuple-element.191) | copy-start | bytes 589828
  60.6 20.7 %copy-start.8 = (f32[768,2,32]{2,0,1:T(8,128)S(1)}, f32[768,2,32]{2,0,1:T(8,128)}, u32[]{:S(2)}) copy-start(f32[768,2,32]{2,0,1:T(8,128)} %get-tuple-element.192) | copy-start | bytes 589828
  60.6 20.7 %copy-start.9 = (f32[768,2,32]{2,0,1:T(8,128)S(1)}, f32[768,2,32]{2,0,1:T(8,128)}, u32[]{:S(2)}) copy-start(f32[768,2,32]{2,0,1:T(8,128)} %get-tuple-element.193) | copy-start | bytes 589828
  60.6 20.7 %copy-start.14 = (f32[768,64]{1,0:T(8,128)S(1)}, f32[768,64]{1,0:T(8,128)}, u32[]{:S(2)}) copy-start(f32[768,64]{1,0:T(8,128)} %copy.29) | copy-start | bytes 589828
  60.6 20.7 %copy-start.15 = (f32[768,64]{1,0:T(8,128)S(1)}, f32[768,64]{1,0:T(8,128)}, u32[]{:S(2)}) copy-start(f32[768,64]{1,0:T(8,128)} %copy.28) | copy-start | bytes 589828
  60.6 20.7 %copy-start.16 = (f32[768,64]{1,0:T(8,128)S(1)}, f32[768,64]{1,0:T(8,128)}, u32[]{:S(2)}) copy-start(f32[768,64]{1,0:T(8,128)} %copy.31) | copy-start | bytes 589828
  60.6 20.7 %copy-start.17 = (f32[768,64]{1,0:T(8,128)S(1)}, f32[768,64]{1,0:T(8,128)}, u32[]{:S(2)}) copy-start(f32[768,64]{1,0:T(8,128)} %copy.30) | copy-start | bytes 589828
  88.4 6.4 %copy-start.1 = (f32[1536,768,2]{1,0,2:T(8,128)S(1)}, f32[1536,768,2]{1,0,2:T(8,128)}, u32[]{:S(2)}) copy-start(f32[1536,768,2]{1,0,2:T(8,128)} %get-tuple-element.271) | copy-start | bytes 28311556 | tf_op jit(solution)/shard_map/while
  103.0 6.4 %copy-start.1 = (f32[1536,768,2]{1,0,2:T(8,128)S(1)}, f32[1536,768,2]{1,0,2:T(8,128)}, u32[]{:S(2)}) copy-start(f32[1536,768,2]{1,0,2:T(8,128)} %get-tuple-element.271) | copy-start | bytes 28311556 | tf_op jit(solution)/shard_map/while
  111.8 2.7 %copy-start.24 = (pred[128,384]{0,1:T(8,128)(4,1)S(1)}, pred[128,384]{0,1:T(8,128)(4,1)}, u32[]{:S(2)}) copy-start(pred[128,384]{0,1:T(8,128)(4,1)} %abs_compare_fusion) | copy-start | bytes 147460
  111.8 3.2 %copy-start.22 = (bf16[768,256]{1,0:T(8,128)(2,1)S(1)}, bf16[768,256]{1,0:T(8,128)(2,1)}, u32[]{:S(2)}) copy-start(bf16[768,256]{1,0:T(8,128)(2,1)} %convolution_convert_fusion.3) | copy-start | bytes 1179652
  111.8 3.3 %copy-start.11 = (bf16[768,128]{1,0:T(8,128)(2,1)S(1)}, bf16[768,128]{1,0:T(8,128)(2,1)}, u32[]{:S(2)}) copy-start(bf16[768,128]{1,0:T(8,128)(2,1)} %copy-done.10) | copy-start | bytes 589828
  111.8 3.3 %copy-start.13 = (bf16[768,128]{1,0:T(8,128)(2,1)S(1)}, bf16[768,128]{1,0:T(8,128)(2,1)}, u32[]{:S(2)}) copy-start(bf16[768,128]{1,0:T(8,128)(2,1)} %copy-done.12) | copy-start | bytes 589828
  116.1 0.7 copy-start.26
  117.5 1.3 copy-start.18
  118.8 1.9 copy-start.2
Sparse Core Ops, SparseCore 0:
  124.2 60.8 reduce-scatter.1
where the time goes:
time: 195 us; the launch traced here: 194 us
  waiting for transfers between devices  61 us (31%)
  blocking collectives  38.9 us (20%)
  matrix products  34.5 us (18%)
  other arithmetic  30.3 us (16%)
  between operations  13.9 us (7%)
  local copies, waits for them, and re-layouts  8.42 us (4%)
  starting transfers between devices  6.86 us (4%)
    reduce_scatter x1, waiting for transfers between devices, shards(): lax.psum_scatter(jnp.concatenate([jnp.dot(grid_result, grid_out_weight, p...  61 us
    all_gather x1, blocking collectives, shards(): lax.all_gather(keys, 'sp', axis=0, tiled=True)  21.4 us
    all_gather x1, blocking collectives, shards(): lax.all_gather(values, 'sp', axis=0, tiled=True)  17.5 us
    dot_general x6, matrix products, project(): jnp.dot(normed, weight, preferred_element_type=jnp.float32)  13.2 us
    dot_general x2, matrix products, absorb(): jnp.einsum('qhgd,shd->hgqs', queries, pieces[0], preferred_element_type=j...  12.2 us
    reduce_sum x2, other arithmetic, absorb(): totals = totals * factor + jnp.sum(weights, axis=-1)  10.7 us
    ppermute x1, starting transfers between devices, padded(): lax.ppermute(lax.slice_in_dim(block, block.shape[dim] - width, None, axis...  5.58 us
    dot_general x2, matrix products, absorb(): jnp.einsum('hgqs,shd->hgqd', weights.astype(jnp.bfloat16), pieces[1], pre...  4.15 us
  transfers between devices with their start and end apart: 3, of which 1 were waited for; matrix products, arithmetic and copies ran while one was open for 27% of the time, Pallas kernels for 0%

commit v1 on v0

v1 whole, which is shorter than its diff:
```python
import functools
import math

import jax
import jax.numpy as jnp
import numpy as np
from jax import lax
from jax.experimental import pallas as pl
from jax.experimental.pallas import tpu as pltpu
from jax.sharding import PartitionSpec as P

HEAD = 128
WINDOW = 128
GRID_W = 64
EPSILON = 1e-06
ROPE_BASE = 10000.0
MASKED = -1e30
MIB = 1 << 20

bf16 = jnp.bfloat16
f32 = jnp.float32
ROWS_T = (((1,), (1,)), ((), ()))


def dot(a, b):
    return jnp.dot(a, b, preferred_element_type=f32)


def turn_tables(total_rows, seq_devices):
    half = HEAD // 2
    quarter = half // 2
    inverse = (ROPE_BASE ** (-np.arange(0, half, 2, dtype=np.float32) / np.float32(half))).astype(np.float32)

    def tables(count, first):
        angles = np.arange(count, dtype=np.float32)[:, None] * inverse
        out = np.zeros((3, count, HEAD), np.float32)
        base = 0 if first else half
        out[0, :, base : base + quarter] = np.cos(angles)
        out[0, :, base + quarter : base + half] = np.cos(angles)
        out[1, :, base : base + quarter] = -np.sin(angles)
        out[2, :, base + quarter : base + half] = np.sin(angles)
        return out

    rows = tables(total_rows // GRID_W, True)
    rows = rows.reshape(3, seq_devices, -1, HEAD).transpose(1, 0, 2, 3)
    return rows, tables(GRID_W, False)


def norm_turn(part, gain, row_tab, col_tab, first_row, grid_rows):
    x = part.astype(bf16).astype(f32)
    x = x * lax.rsqrt(jnp.mean(x * x, axis=-1, keepdims=True) + EPSILON) * gain

    def table(k):
        rows = row_tab[k, pl.ds(first_row, grid_rows), :]
        return (rows[:, None, :] + col_tab[k][None, :, :]).reshape(grid_rows * GRID_W, HEAD)

    quarter = HEAD // 4
    return (
        x * table(0)
        + pltpu.roll(x, HEAD - quarter, 1) * table(1)
        + pltpu.roll(x, quarter, 1) * table(2)
    )


def kv_body(tile, steps, tok, gain, wk, wv, lwk, lwv, kgain, row_tab, col_tab, normed, up, down, lkv):
    step = pl.program_id(0)
    x = tok[...].astype(f32)
    n = (x * lax.rsqrt(jnp.mean(x * x, axis=-1, keepdims=True) + EPSILON) * gain[...]).astype(bf16)
    normed[...] = n
    y = dot(n, jnp.concatenate([wk[...], wv[...], lwk[...], lwv[...]], axis=1))
    grid_rows = tile // GRID_W
    keys = norm_turn(y[:, :HEAD], kgain[...], row_tab, col_tab, step * grid_rows, grid_rows)
    pair = jnp.concatenate([keys, y[:, HEAD : 2 * HEAD]], axis=1).astype(bf16)
    local = y[:, 2 * HEAD :].astype(bf16)
    rows = pl.ds(step * tile, tile)
    up[rows, :] = pair
    down[rows, :] = pair
    lkv[rows, :] = local

    @pl.when(step == steps - 1)
    def _():
        up[pl.ds(steps * tile, WINDOW), :] = local[tile - WINDOW :]

    @pl.when(step == 0)
    def _():
        down[pl.ds(steps * tile, WINDOW), :] = local[:WINDOW]


def q_body(tile, steps, normed, wq, lwq, qgain, row_tab, col_tab, q, lq):
    weights = jnp.concatenate([wq[...], lwq[...]], axis=1)
    heads = wq.shape[1] // HEAD
    grid_rows = tile // GRID_W
    for step in range(steps):
        rows = pl.ds(step * tile, tile)
        y = dot(normed[rows, :], weights)
        for h in range(heads):
            part = y[:, h * HEAD : (h + 1) * HEAD]
            turned = norm_turn(part, qgain[...], row_tab, col_tab, step * grid_rows, grid_rows)
            q[pl.ds(h * steps * tile + step * tile, tile), :] = turned.astype(bf16)
        lq[rows, :] = y[:, heads * HEAD :].astype(bf16)


def local_body(blocks, total_rows, info, sink, lq, lkv, low, high, out):
    offset = info[0] * (blocks * WINDOW)
    scale = HEAD ** (-0.5)
    row = lax.broadcasted_iota(jnp.int32, (WINDOW, 3 * WINDOW), 0)
    col = lax.broadcasted_iota(jnp.int32, (WINDOW, 3 * WINDOW), 1)
    band = jnp.abs(col - WINDOW - row) <= WINDOW
    pieces = [low[...]] + [lkv[pl.ds(i * WINDOW, WINDOW), :] for i in range(blocks)] + [high[...]]
    heads = lq.shape[1] // HEAD
    for i in range(blocks):
        keys = jnp.concatenate([p[:, :HEAD] for p in pieces[i : i + 3]], axis=0)
        values = jnp.concatenate([p[:, HEAD:] for p in pieces[i : i + 3]], axis=0)
        valid = band
        if i == 0 or i == blocks - 1:
            pos = offset + (i - 1) * WINDOW + col
            valid = band & (pos >= 0) & (pos < total_rows)
        for h in range(heads):
            query = lq[pl.ds(i * WINDOW, WINDOW), h * HEAD : (h + 1) * HEAD]
            s = lax.dot_general(query, keys, ROWS_T, preferred_element_type=f32) * scale
            s = jnp.where(valid, s, MASKED)
            top = jnp.maximum(jnp.max(s, axis=-1, keepdims=True), sink[0, h])
            p = jnp.exp(s - top)
            den = jnp.sum(p, axis=-1, keepdims=True) + jnp.exp(sink[0, h] - top)
            o = dot(p.astype(bf16), values) / den
            out[pl.ds(i * WINDOW, WINDOW), h * HEAD : (h + 1) * HEAD] = o.astype(bf16)


def attend_body(tile, spans, first, last, *refs):
    q = refs[0]
    kvs = refs[1 : 1 + len(spans)]
    rest = refs[1 + len(spans) :]
    if not first:
        m_in, acc_in, rest = rest[0], rest[1], rest[2:]
    rows_all = q.shape[0]
    ones = [jnp.ones((span, HEAD), bf16) for span in spans]
    for t in range(rows_all // tile):
        rows = pl.ds(t * tile, tile)
        query = q[rows, :]
        m = None if first else m_in[rows, :]
        acc = None if first else acc_in[rows, :]
        for kv, span, one in zip(kvs, spans, ones):
            keys = kv[pl.ds(0, span), :HEAD]
            values = jnp.concatenate([kv[pl.ds(0, span), HEAD:], one], axis=1)
            s = lax.dot_general(query, keys, ROWS_T, preferred_element_type=f32)
            top = jnp.broadcast_to(jnp.max(s, axis=-1, keepdims=True), (tile, HEAD))
            new = top if m is None else jnp.maximum(m, top)
            p = jnp.exp2(s - jnp.concatenate([new] * (span // HEAD), axis=1)).astype(bf16)
            add = dot(p, values)
            if m is None:
                acc = add
            else:
                factor = jnp.exp2(m - new)
                acc = acc * jnp.concatenate([factor, factor], axis=1) + add
            m = new
        if last:
            o = (acc[:, :HEAD] / acc[:, HEAD:]).astype(bf16)
            row_count = rest[0].shape[0]
            h, r = divmod(t * tile, row_count)
            rest[0][pl.ds(r, tile), h * HEAD : (h + 1) * HEAD] = o
        else:
            rest[0][rows, :] = m
            rest[1][rows, :] = acc


def vmem(count):
    return [pl.BlockSpec(memory_space=pltpu.VMEM)] * count


def sds(shape, dtype):
    return jax.ShapeDtypeStruct(shape, dtype)


def cost(flops, transcendentals=0, bytes_accessed=0):
    return pl.CostEstimate(flops=int(flops), transcendentals=int(transcendentals), bytes_accessed=int(bytes_accessed))


def attend(q, blocks, state, last, row_count):
    rows, tile = q.shape[0], 256
    spans = tuple(b[1] for b in blocks)
    operands = [q] + [b[0] for b in blocks] + ([] if state is None else list(state))
    if last:
        shape = sds((row_count, rows // row_count * HEAD), bf16)
    else:
        shape = (sds((rows, HEAD), f32), sds((rows, 2 * HEAD), f32))
    keys = sum(spans)
    return pl.pallas_call(
        functools.partial(attend_body, tile, spans, state is None, last),
        out_shape=shape,
        in_specs=vmem(len(operands)),
        out_specs=pl.BlockSpec(memory_space=pltpu.VMEM) if last else tuple(vmem(2)),
        compiler_params=pltpu.CompilerParams(vmem_limit_bytes=24 * MIB),
        cost_estimate=cost(rows * keys * HEAD * 8, rows * keys),
        name="attend",
    )(*operands)


def shards(
    tokens,
    norm_gain,
    grid_query_weight,
    grid_key_weight,
    grid_value_weight,
    grid_query_gain,
    grid_key_gain,
    local_query_weight,
    local_key_weight,
    local_value_weight,
    sink_logit,
    grid_out_weight,
    local_out_weight,
):
    row_count, width = tokens.shape
    n_sp = lax.axis_size("sp")
    n_tp = lax.axis_size("tp")
    total_rows = row_count * n_sp
    sp = lax.axis_index("sp")
    tp = lax.axis_index("tp")
    heads = grid_query_weight.shape[1] // HEAD
    row_np, col_np = turn_tables(total_rows, n_sp)
    row_tab = lax.dynamic_index_in_dim(jnp.asarray(row_np), sp, 0, keepdims=False)
    col_tab = jnp.asarray(col_np)

    tile = 256
    steps = row_count // tile
    fixed = lambda *shape: pl.BlockSpec(shape, lambda i: (0,) * len(shape))
    grid_rows = row_count // GRID_W
    normed, up, down, lkv = pl.pallas_call(
        functools.partial(kv_body, tile, steps),
        grid=(steps,),
        out_shape=(
            sds((row_count, width), bf16),
            sds((row_count + WINDOW, 2 * HEAD), bf16),
            sds((row_count + WINDOW, 2 * HEAD), bf16),
            sds((row_count, 2 * HEAD), bf16),
        ),
        in_specs=[
            pl.BlockSpec((tile, width), lambda i: (i, 0)),
            fixed(1, width),
            fixed(width, HEAD),
            fixed(width, HEAD),
            fixed(width, HEAD),
            fixed(width, HEAD),
            fixed(1, HEAD),
            fixed(3, grid_rows, HEAD),
            fixed(3, GRID_W, HEAD),
        ],
        out_specs=(
            pl.BlockSpec((tile, width), lambda i: (i, 0)),
            fixed(row_count + WINDOW, 2 * HEAD),
            fixed(row_count + WINDOW, 2 * HEAD),
            fixed(row_count, 2 * HEAD),
        ),
        compiler_params=pltpu.CompilerParams(vmem_limit_bytes=24 * MIB),
        cost_estimate=cost(2 * row_count * width * 4 * HEAD, 0, 8 * MIB),
        name="keys",
    )(
        tokens,
        norm_gain.reshape(1, width),
        grid_key_weight,
        grid_value_weight,
        local_key_weight,
        local_value_weight,
        grid_key_gain.reshape(1, HEAD),
        row_tab,
        col_tab,
    )

    forward = [(i, (i + 1) % n_sp) for i in range(n_sp)]
    backward = [(t, s) for s, t in forward]
    from_low = lax.ppermute(up, "sp", forward)
    from_high = lax.ppermute(down, "sp", backward)

    fold = HEAD ** (-0.5) * math.log2(math.e)
    q, lq = pl.pallas_call(
        functools.partial(q_body, tile, steps),
        out_shape=(sds((heads * row_count, HEAD), bf16), sds((row_count, heads * HEAD), bf16)),
        in_specs=vmem(6),
        out_specs=tuple(vmem(2)),
        compiler_params=pltpu.CompilerParams(vmem_limit_bytes=24 * MIB),
        cost_estimate=cost(2 * row_count * width * 4 * HEAD, 0, 6 * MIB),
        name="queries",
    )(normed, grid_query_weight, local_query_weight, (grid_query_gain * fold).reshape(1, HEAD), row_tab, col_tab)

    state = attend(q, [(up, row_count)], None, False, row_count)

    low, high = from_low, from_high
    pending = []
    for _ in range(1, (n_sp - 1) // 2):
        next_low = lax.ppermute(low[:row_count], "sp", forward)
        next_high = lax.ppermute(high[:row_count], "sp", backward)
        state = attend(q, [(low, row_count), (high, row_count)], state, False, row_count)
        low, high = next_low, next_high
    half = row_count // 2
    far_low = lax.ppermute(low[:half], "sp", forward)
    far_high = lax.ppermute(high[half:row_count], "sp", backward)

    local_out = pl.pallas_call(
        functools.partial(local_body, row_count // WINDOW, total_rows),
        out_shape=sds((row_count, heads * HEAD), bf16),
        in_specs=[pl.BlockSpec(memory_space=pltpu.SMEM)] * 2 + vmem(4),
        out_specs=pl.BlockSpec(memory_space=pltpu.VMEM),
        compiler_params=pltpu.CompilerParams(vmem_limit_bytes=24 * MIB),
        cost_estimate=cost(heads * row_count * 3 * WINDOW * HEAD * 8, heads * row_count * 3 * WINDOW),
        name="banded",
    )(
        sp.reshape(1).astype(jnp.int32),
        sink_logit.reshape(1, heads),
        lq,
        lkv,
        lax.slice_in_dim(from_low, row_count, row_count + WINDOW),
        lax.slice_in_dim(from_high, row_count, row_count + WINDOW),
    )
    state = attend(q, [(low, row_count), (high, row_count)], state, False, row_count)
    grid_out = attend(q, [(far_low, half), (far_high, half)], state, True, row_count)

    flip = lambda bit: [(i, i ^ bit) for i in range(n_tp)]
    take = lambda v, i, axis: lax.dynamic_index_in_dim(v, i, axis, keepdims=False)
    b0, b1, b2 = tp % 2, (tp // 2) % 2, tp // 4
    piece = row_count // n_tp
    both = jnp.concatenate([grid_out, local_out], axis=1)
    weights = jnp.concatenate([grid_out_weight, local_out_weight], axis=0)
    partial = dot(both, weights).reshape(2, 2, 2, piece, width)
    got = lax.ppermute(take(partial, 1 - b0, 2).astype(bf16), "tp", flip(1))
    acc = take(partial, b0, 2) + got.astype(f32)
    side = width // 2
    left, right = acc[..., :side], acc[..., side:]
    got_l = lax.ppermute(take(left, 1 - b1, 1).astype(bf16), "tp", flip(2))
    got_r = lax.ppermute(take(right, 1 - b2, 0).astype(bf16), "tp", flip(4))
    left = take(left, b1, 1) + got_l.astype(f32)
    right = take(right, b2, 0) + got_r.astype(f32)
    got_l = lax.ppermute(take(left, 1 - b2, 0).astype(bf16), "tp", flip(4))
    got_r = lax.ppermute(take(right, 1 - b1, 0).astype(bf16), "tp", flip(2))
    left = take(left, b2, 0) + got_l.astype(f32)
    right = take(right, b1, 0) + got_r.astype(f32)
    return jnp.concatenate([left, right], axis=1).astype(bf16)


def solution(mesh):
    in_specs = (
        P("sp", None),
        P(),
        P(None, "tp"),
        P(None, "tp"),
        P(None, "tp"),
        P(),
        P(),
        P(None, "tp"),
        P(None, "tp"),
        P(None, "tp"),
        P("tp"),
        P("tp", None),
        P("tp", None),
    )
    out_specs = P(("sp", "tp"), None)
    return jax.shard_map(shards, mesh=mesh, in_specs=in_specs, out_specs=out_specs, check_vma=False)
```

time: 195 us -> 88 us (0.45)
  blocking collectives: 38.9 us -> 0 us
  waiting for transfers between devices: 61 us -> 27 us
  matrix products: 34.5 us -> 1.8 us
  other arithmetic: 30.3 us -> 4.42 us
  Pallas kernels: 0 us -> 18.1 us
  between operations: 13.9 us -> 0.29 us
  local copies, waits for them, and re-layouts: 8.42 us -> 19 us
  starting transfers between devices: 6.86 us -> 16.9 us
    reduce_scatter x1 -> x0, waiting for transfers between devices: 61 us -> none  [shards(): lax.psum_scatter(jnp.concatenate([jnp.dot(grid_result, grid_out_weight, p...]
    all_gather x2 -> x0, blocking collectives: 38.9 us -> none  [the longest x1 21.4 us: shards(): lax.all_gather(keys, 'sp', axis=0, tiled=True)]
    dot_general x14 -> x1, matrix products: 34.5 us -> 1.8 us  [dot(): return jnp.dot(a, b, preferred_element_type=f32)]
    ppermute x2 -> x9, waiting for transfers between devices: 0.01 us -> 27 us  [the longest x1 7.56 us: shards(): got_r = lax.ppermute(take(right, 1 - b2, 0).astype(bf16), 'tp', flip(4))]
    pallas_call x0 -> x6, Pallas kernels: none -> 18.1 us  [the longest x3 7.95 us: attend(): pl.pallas_call(functools.partial(attend_body, tile, spans, state is None,...]
    unnamed x62 -> x40, local copies, waits for them, and re-layouts: 1.91 us -> 16.1 us
    reduce_sum x4 -> x0, other arithmetic: 14 us -> none  [the longest x2 10.7 us: absorb(): totals = totals * factor + jnp.sum(weights, axis=-1)]
    ppermute x2 -> x9, starting transfers between devices: 6.86 us -> 16.9 us  [the longest x1 5.09 us: shards(): from_high = lax.ppermute(down, 'sp', backward)]
  transfers between devices with their start and end apart: 3 -> 9, of which waited for: 1 -> 7; matrix products, arithmetic and copies ran while one was open for 27% -> 2% of each run, Pallas kernels for 0% -> 12%
where the time goes in v1:
time: 88 us; the launch traced here: 87.4 us
  waiting for transfers between devices  27 us (31%)
  local copies, waits for them, and re-layouts  19 us (22%)
  Pallas kernels  18.1 us (21%)
  starting transfers between devices  16.9 us (19%)
  other arithmetic  4.42 us (5%)
  matrix products  1.8 us (2%)
    unnamed x40, local copies, waits for them, and re-layouts  16.1 us
    pallas_call x3, Pallas kernels, attend(): pl.pallas_call(functools.partial(attend_body, tile, spans, state is None,...  7.95 us
    ppermute x1, waiting for transfers between devices, shards(): got_r = lax.ppermute(take(right, 1 - b2, 0).astype(bf16), 'tp', flip(4))  7.56 us
    ppermute x1, waiting for transfers between devices, shards(): from_low = lax.ppermute(up, 'sp', forward)  6.42 us
    ppermute x1, starting transfers between devices, shards(): from_high = lax.ppermute(down, 'sp', backward)  5.09 us
    ppermute x1, waiting for transfers between devices, shards(): from_high = lax.ppermute(down, 'sp', backward)  4.5 us
    ppermute x1, starting transfers between devices, shards(): far_high = lax.ppermute(high[half:row_count], 'sp', backward)  4.23 us
    pallas_call x1, Pallas kernels, shards(): pl.pallas_call(functools.partial(kv_body, tile, steps), grid=(steps,), ou...  4.19 us
  transfers between devices with their start and end apart: 9, of which 7 were waited for; matrix products, arithmetic and copies ran while one was open for 2% of the time, Pallas kernels for 12%

profile of v1, /device:TPU:0, one launch (start us, length us, event | category | flops | bytes accessed | tf_op | source)
XLA Modules:
  0.0 87.4 jit_solution(14791914670998502010)
XLA Ops:
  0.0 0.7 dynamic-slice_bitcast_fusion.row_tab
  0.7 1.9 %copy-done = bf16[768,2048]{1,0:T(8,128)(2,1)S(1)} copy-done((bf16[768,2048]{1,0:T(8,128)(2,1)S(1)}, bf16[768,2048]{1,0:T(8,128)(2,1)}, u32[]{:S(2)}) %copy-start) | copy-done | bytes 3145752
  2.6 1.0 %copy-done.3 = bf16[2048,128]{1,0:T(8,128)(2,1)S(1)} copy-done((bf16[2048,128]{1,0:T(8,128)(2,1)S(1)}, bf16[2048,128]{1,0:T(8,128)(2,1)}, u32[]{:S(2)}) %copy-start.3) | copy-done | bytes 524312
  3.7 1.0 %copy-done.4 = bf16[2048,128]{1,0:T(8,128)(2,1)S(1)} copy-done((bf16[2048,128]{1,0:T(8,128)(2,1)S(1)}, bf16[2048,128]{1,0:T(8,128)(2,1)}, u32[]{:S(2)}) %copy-start.4) | copy-done | bytes 524312
  4.7 1.0 %copy-done.5 = bf16[2048,128]{1,0:T(8,128)(2,1)S(1)} copy-done((bf16[2048,128]{1,0:T(8,128)(2,1)S(1)}, bf16[2048,128]{1,0:T(8,128)(2,1)}, u32[]{:S(2)}) %copy-start.5) | copy-done | bytes 524312
  5.8 1.0 %copy-done.6 = bf16[2048,128]{1,0:T(8,128)(2,1)S(1)} copy-done((bf16[2048,128]{1,0:T(8,128)(2,1)S(1)}, bf16[2048,128]{1,0:T(8,128)(2,1)}, u32[]{:S(2)}) %copy-start.6) | copy-done | bytes 524312
  6.8 0.7 copy-done.7
  7.5 0.7 copy-done.8
  8.2 0.9 %copy-done.10 = f32[3,64,128]{2,1,0:T(8,128)S(1)} copy-done((f32[3,64,128]{2,1,0:T(8,128)S(1)}, f32[3,64,128]{2,1,0:T(8,128)}, u32[]{:S(2)}) %copy-start.10) | copy-done | bytes 98328
  9.1 4.2 %keys.1 = (bf16[768,2048]{1,0:T(8,128)(2,1)S(1)}, bf16[896,256]{1,0:T(8,128)(2,1)S(1)}, bf16[896,256]{1,0:T(8,128)(2,1)}, bf16[768,256]{1,0:T(8,128)(2,1)S(1)}) custom-call(bf16[768,2048]{1,0:T(8,128)(2,1)S(1)} %copy-done, f32[1,2048]{1,0:T(1,128)S(1)} %bitcast.37, bf16[2048,128]{1,0:T(8,128)(2,1)S(1)} %copy-done.3, bf16[2048,128]{1,0:T(8,128)(2,1)S(1)} %copy-done.4, ...), custom_call_target="tpu_custom_call" | custom-call | flops 1610612736 | bytes 8388608 | tf_op jit(solution)/shard_map/keys/pallas_call | solution.py:228
  13.2 1.6 %copy-done.12 = bf16[768,2048]{1,0:T(8,128)(2,1)} copy-done((bf16[768,2048]{1,0:T(8,128)(2,1)}, bf16[768,2048]{1,0:T(8,128)(2,1)S(1)}, u32[]{:S(2)}) %copy-start.12) | copy-done | bytes 3145752
  14.9 0.7 copy-done.14
  15.6 5.1 %collective-permute-start.2 = (bf16[896,256]{1,0:T(8,128)(2,1)}, bf16[896,256]{1,0:T(8,128)(2,1)S(1)}, u32[]{:S(2)}, u32[]{:S(2)}) collective-permute-start(bf16[896,256]{1,0:T(8,128)(2,1)} %get-tuple-element.18), channel_id=1, source_target_pairs={{8,0},{16,8},{24,16},{0,24},{9,1},{17,9},{25,17},{1,25},{10,2},{18... | collective-permute-start | bytes 1376264 | tf_op jit(solution)/shard_map/ppermute | solution.py:272
  20.7 0.0 copy-start.11
  20.7 0.9 %copy-done.11 = f32[3,64,128]{2,1,0:T(8,128)S(1)} copy-done((f32[3,64,128]{2,1,0:T(8,128)S(1)}, f32[3,64,128]{2,1,0:T(8,128)}, u32[]{:S(2)}) %copy-start.11) | copy-done | bytes 98328
  21.6 1.9 %copy-done.13 = bf16[768,2048]{1,0:T(8,128)(2,1)S(1)} copy-done((bf16[768,2048]{1,0:T(8,128)(2,1)S(1)}, bf16[768,2048]{1,0:T(8,128)(2,1)}, u32[]{:S(2)}) %copy-start.13) | copy-done | bytes 3145752
  23.5 2.1 %queries.1 = (bf16[1536,128]{1,0:T(8,128)(2,1)S(1)}, bf16[768,256]{1,0:T(8,128)(2,1)S(1)}) custom-call(bf16[768,2048]{1,0:T(8,128)(2,1)S(1)} %copy-done.13, bf16[2048,256]{1,0:T(8,128)(2,1)S(1)} %copy-done.1, bf16[2048,256]{1,0:T(8,128)(2,1)S(1)} %copy-done.2, f32[1,128]{1,0:T(1,128)S(1)} %multiply_bitcast_fusion.qgain, ...), custom_call_target="tpu_custom_call" | custom-call | flops 1610612736 | bytes 6291456 | tf_op jit(solution)/shard_map/queries/pallas_call | solution.py:275
  25.6 0.0 copy-start.9
  25.7 1.7 %attend.3 = (f32[1536,128]{1,0:T(8,128)S(1)}, f32[1536,256]{1,0:T(8,128)S(1)}) custom-call(bf16[1536,128]{1,0:T(8,128)(2,1)S(1)} %get-tuple-element.16.refs_0_, bf16[896,256]{1,0:T(8,128)(2,1)S(1)} %get-tuple-element.17.refs_1_), custom_call_target="tpu_custom_call" | custom-call | flops 1207959552 | tf_op jit(solution)/shard_map/attend/pallas_call | solution.py:187
  27.4 4.5 %collective-permute-done.2.refs_2_ = bf16[896,256]{1,0:T(8,128)(2,1)S(1)} collective-permute-done((bf16[896,256]{1,0:T(8,128)(2,1)}, bf16[896,256]{1,0:T(8,128)(2,1)S(1)}, u32[]{:S(2)}, u32[]{:S(2)}) %collective-permute-start.2) | collective-permute-done | bytes 458784 | tf_op jit(solution)/shard_map/ppermute | solution.py:272
  31.9 4.2 %collective-permute-start.3 = (bf16[384,256]{1,0:T(8,128)(2,1)S(1)}, bf16[384,256]{1,0:T(8,128)(2,1)S(1)}, u32[]{:S(2)}, u32[]{:S(2)}) collective-permute-start(bf16[384,256]{1,0:T(8,128)(2,1)S(1)} %slice.25), channel_id=1, source_target_pairs={{8,0},{16,8},{24,16},{0,24},{9,1},{17,9},{25,17},{1,25},{10,2},{18... | collective-permute-start | bytes 589832 | tf_op jit(solution)/shard_map/ppermute | solution.py:296
  36.2 6.4 %collective-permute-done.refs_1_ = bf16[896,256]{1,0:T(8,128)(2,1)S(1)} collective-permute-done((bf16[896,256]{1,0:T(8,128)(2,1)S(1)}, bf16[896,256]{1,0:T(8,128)(2,1)S(1)}, u32[]{:S(2)}, u32[]{:S(2)}) %collective-permute-start) | collective-permute-done | bytes 458784 | tf_op jit(solution)/shard_map/ppermute | solution.py:271
  42.6 1.8 %collective-permute-start.1 = (bf16[384,256]{1,0:T(8,128)(2,1)S(1)}, bf16[384,256]{1,0:T(8,128)(2,1)S(1)}, u32[]{:S(2)}, u32[]{:S(2)}) collective-permute-start(bf16[384,256]{1,0:T(8,128)(2,1)S(1)} %slice.24), channel_id=1, source_target_pairs={{0,8},{8,16},{16,24},{24,0},{1,9},{9,17},{17,25},{25,1},{2,10},{10... | collective-permute-start | bytes 589832 | tf_op jit(solution)/shard_map/ppermute | solution.py:295
  44.4 3.8 %banded.1 = bf16[768,256]{1,0:T(8,128)(2,1)S(1)} custom-call(s32[1]{0:T(128)} %bitcast.4.info, f32[1,2]{1,0:T(1,128)S(1)} %bitcast.39, bf16[768,256]{1,0:T(8,128)(2,1)S(1)} %get-tuple-element.23.lq, bf16[768,256]{1,0:T(8,128)(2,1)S(1)} %copy-done.15, bf16[128,256]{1,0:T(8,128)(2,1)S(1)} %slice.26.low, bf16[128,256]{1,0:T(8,128)(2,1)S(1)} %slice.27.high), custom_call_target="tpu_custom_call" | custom-call | flops 603979776 | tf_op jit(solution)/shard_map/banded/pallas_call | solution.py:298
  48.2 3.1 %attend.4 = (f32[1536,128]{1,0:T(8,128)S(1)}, f32[1536,256]{1,0:T(8,128)S(1)}) custom-call(bf16[1536,128]{1,0:T(8,128)(2,1)S(1)} %get-tuple-element.16.refs_0_, bf16[896,256]{1,0:T(8,128)(2,1)S(1)} %collective-permute-done.refs_1_, bf16[896,256]{1,0:T(8,128)(2,1)S(1)} %collective-permute-done.2.refs_2_, f32[1536,128]{1,0:T(8,128)S(1)} %get-tuple-element.19.refs_3_, ...), custom_call_target="tpu_custom_call" | custom-call | flops 2415919104 | tf_op jit(solution)/shard_map/attend/pallas_call | solution.py:187
  51.4 0.0 copy-start.17
  51.4 0.0 copy-start.18
  51.4 3.1 %attend.5 = bf16[768,256]{1,0:T(8,128)(2,1)S(1)} custom-call(bf16[1536,128]{1,0:T(8,128)(2,1)S(1)} %get-tuple-element.16.refs_0_, bf16[384,256]{1,0:T(8,128)(2,1)S(1)} %collective-permute-done.1.refs_1_, bf16[384,256]{1,0:T(8,128)(2,1)S(1)} %collective-permute-done.3.refs_2_, f32[1536,128]{1,0:T(8,128)S(1)} %get-tuple-element.21.refs_3_, ...), custom_call_target="tpu_custom_call" | custom-call | flops 1207959552 | tf_op jit(solution)/shard_map/attend/pallas_call | solution.py:187
  54.5 1.8 %fusion = f32[768,2048]{1,0:T(8,128)S(1)} fusion(bf16[256,2048]{1,0:T(8,128)(2,1)S(1)} %copy-done.17, bf16[256,2048]{1,0:T(8,128)(2,1)S(1)} %copy-done.18, bf16[768,256]{1,0:T(8,128)(2,1)S(1)} %banded.1, bf16[768,256]{1,0:T(8,128)(2,1)S(1)} %attend.5), kind=kOutput, calls=%fused_computation.2 | convolution fusion | flops 1616379904 | bytes 9175040 | tf_op jit(solution)/shard_map/dot_general | solution.py:26
  56.3 2.6 %copy-done.16 = f32[768,2048]{1,0:T(8,128)} copy-done((f32[768,2048]{1,0:T(8,128)}, f32[768,2048]{1,0:T(8,128)S(1)}, u32[]{:S(2)}) %copy-start.16) | copy-done | bytes 6291480
  59.0 0.2 fusion.4
  59.2 0.1 collective-permute-start.4
  59.3 3.4 %collective-permute-done.4 = bf16[2,2,96,2048]{3,2,1,0:T(8,128)(2,1)S(1)} collective-permute-done((bf16[2,2,96,2048]{3,2,1,0:T(8,128)(2,1)S(1)}, bf16[2,2,96,2048]{3,2,1,0:T(8,128)(2,1)S(1)}, u32[]{:S(2)}, u32[]{:S(2)}) %collective-permute-start.4) | collective-permute-done | bytes 1572896 | tf_op jit(solution)/shard_map/ppermute | solution.py:324
  62.7 2.4 %bitcast_add_fusion = f32[2,2,96,2048]{3,2,1,0:T(8,128)S(1)} fusion(bf16[2,2,96,2048]{3,2,1,0:T(8,128)(2,1)S(1)} %collective-permute-done.4, f32[2,2,2,96,2048]{4,3,2,1,0:T(8,128)} %bitcast.41, s32[]{:T(128)S(6)} %select_n.50), kind=kLoop, calls=%fused_computation.1 | loop fusion | flops 1572864 | bytes 7864324 | tf_op jit(solution)/shard_map/add | solution.py:325
  65.1 0.2 fusion.15
  65.3 0.8 fusion.9
  66.1 1.5 %collective-permute-start.7 = (bf16[2,96,1024]{2,1,0:T(8,128)(2,1)}, bf16[2,96,1024]{2,1,0:T(8,128)(2,1)S(1)}, u32[]{:S(2)}, u32[]{:S(2)}) collective-permute-start(bf16[2,96,1024]{2,1,0:T(8,128)(2,1)} %fusion.9), channel_id=1, source_target_pairs={{0,4},{1,5},{2,6},{3,7},{4,0},{5,1},{6,2},{7,3},{8,12},{9,13},{10,... | collective-permute-start | bytes 1179656 | tf_op jit(solution)/shard_map/ppermute | solution.py:329
  67.6 0.8 fusion.8
  68.4 1.5 %collective-permute-start.5 = (bf16[2,96,1024]{2,1,0:T(8,128)(2,1)}, bf16[2,96,1024]{2,1,0:T(8,128)(2,1)}, u32[]{:S(2)}, u32[]{:S(2)}) collective-permute-start(bf16[2,96,1024]{2,1,0:T(8,128)(2,1)} %fusion.8), channel_id=1, source_target_pairs={{0,2},{1,3},{2,0},{3,1},{4,6},{5,7},{6,4},{7,5},{8,10},{9,11},{10,... | collective-permute-start | bytes 1179656 | tf_op jit(solution)/shard_map/ppermute | solution.py:328
  69.9 7.6 %collective-permute-done.7 = bf16[2,96,1024]{2,1,0:T(8,128)(2,1)S(1)} collective-permute-done((bf16[2,96,1024]{2,1,0:T(8,128)(2,1)}, bf16[2,96,1024]{2,1,0:T(8,128)(2,1)S(1)}, u32[]{:S(2)}, u32[]{:S(2)}) %collective-permute-start.7) | collective-permute-done | bytes 393248 | tf_op jit(solution)/shard_map/ppermute | solution.py:329
  77.5 0.1 bitcast_add_fusion.1
  77.6 1.6 %collective-permute-start.8 = (bf16[96,1024]{1,0:T(8,128)(2,1)S(1)}, bf16[96,1024]{1,0:T(8,128)(2,1)S(1)}, u32[]{:S(2)}, u32[]{:S(2)}) collective-permute-start(bf16[96,1024]{1,0:T(8,128)(2,1)S(1)} %fusion.13), channel_id=1, source_target_pairs={{0,2},{1,3},{2,0},{3,1},{4,6},{5,7},{6,4},{7,5},{8,10},{9,11},{10,... | collective-permute-start | bytes 589832 | tf_op jit(solution)/shard_map/ppermute | solution.py:333
  79.1 0.5 collective-permute-done.5
  79.6 1.1 %bitcast_add_fusion.2 = f32[2,96,1024]{2,1,0:T(8,128)S(1)} fusion(bf16[2,96,1024]{2,1,0:T(8,128)(2,1)} %collective-permute-done.5, f32[2,2,96,1024]{3,2,1,0:T(8,128)S(1)} %get-tuple-element.25, s32[]{:T(128)S(6)} %select_n.54), kind=kLoop, calls=%fused_computation.11 | loop fusion | flops 393216 | bytes 1966084 | tf_op jit(solution)/shard_map/add | solution.py:330
  80.7 1.1 %collective-permute-start.6 = (bf16[96,1024]{1,0:T(8,128)(2,1)S(1)}, bf16[96,1024]{1,0:T(8,128)(2,1)S(1)}, u32[]{:S(2)}, u32[]{:S(2)}) collective-permute-start(bf16[96,1024]{1,0:T(8,128)(2,1)S(1)} %fusion.12), channel_id=1, source_target_pairs={{0,4},{1,5},{2,6},{3,7},{4,0},{5,1},{6,2},{7,3},{8,12},{9,13},{10,... | collective-permute-start | bytes 589832 | tf_op jit(solution)/shard_map/ppermute | solution.py:332
  81.9 2.0 %collective-permute-done.8 = bf16[96,1024]{1,0:T(8,128)(2,1)S(1)} collective-permute-done((bf16[96,1024]{1,0:T(8,128)(2,1)S(1)}, bf16[96,1024]{1,0:T(8,128)(2,1)S(1)}, u32[]{:S(2)}, u32[]{:S(2)}) %collective-permute-start.8) | collective-permute-done | bytes 196640 | tf_op jit(solution)/shard_map/ppermute | solution.py:333
  83.9 2.7 %collective-permute-done.6 = bf16[96,1024]{1,0:T(8,128)(2,1)S(1)} collective-permute-done((bf16[96,1024]{1,0:T(8,128)(2,1)S(1)}, bf16[96,1024]{1,0:T(8,128)(2,1)S(1)}, u32[]{:S(2)}, u32[]{:S(2)}) %collective-permute-start.6) | collective-permute-done | bytes 196640 | tf_op jit(solution)/shard_map/ppermute | solution.py:332
  86.6 0.8 pad_maximum_fusion
  (35 shorter events, 0.2 us)
Async XLA Ops:
  0.7 1.9 %copy-start = (bf16[768,2048]{1,0:T(8,128)(2,1)S(1)}, bf16[768,2048]{1,0:T(8,128)(2,1)}, u32[]{:S(2)}) copy-start(bf16[768,2048]{1,0:T(8,128)(2,1)} %tok.1) | copy-start | bytes 9437188
  2.6 1.0 %copy-start.3 = (bf16[2048,128]{1,0:T(8,128)(2,1)S(1)}, bf16[2048,128]{1,0:T(8,128)(2,1)}, u32[]{:S(2)}) copy-start(bf16[2048,128]{1,0:T(8,128)(2,1)} %wk.1) | copy-start | bytes 1572868
  3.7 1.0 %copy-start.4 = (bf16[2048,128]{1,0:T(8,128)(2,1)S(1)}, bf16[2048,128]{1,0:T(8,128)(2,1)}, u32[]{:S(2)}) copy-start(bf16[2048,128]{1,0:T(8,128)(2,1)} %wv.1) | copy-start | bytes 1572868
  4.7 1.0 %copy-start.5 = (bf16[2048,128]{1,0:T(8,128)(2,1)S(1)}, bf16[2048,128]{1,0:T(8,128)(2,1)}, u32[]{:S(2)}) copy-start(bf16[2048,128]{1,0:T(8,128)(2,1)} %lwk.1) | copy-start | bytes 1572868
  5.8 1.0 %copy-start.6 = (bf16[2048,128]{1,0:T(8,128)(2,1)S(1)}, bf16[2048,128]{1,0:T(8,128)(2,1)}, u32[]{:S(2)}) copy-start(bf16[2048,128]{1,0:T(8,128)(2,1)} %lwv.1) | copy-start | bytes 1572868
  6.8 0.7 copy-start.7
  7.5 0.7 copy-start.8
  8.2 0.9 %copy-start.10 = (f32[3,64,128]{2,1,0:T(8,128)S(1)}, f32[3,64,128]{2,1,0:T(8,128)}, u32[]{:S(2)}) copy-start(f32[3,64,128]{2,1,0:T(8,128)} %constant.90.clone.col_tab) | copy-start | bytes 294916
  9.0 11.7 %copy-start.19 = (f32[128]{0:T(128)S(1)}, f32[128]{0:T(128)}, u32[]{:S(2)}) copy-start(f32[128]{0:T(128)} %param.20) | copy-start | bytes 1540
  9.0 11.7 %copy-start.1 = (bf16[2048,256]{1,0:T(8,128)(2,1)S(1)}, bf16[2048,256]{1,0:T(8,128)(2,1)}, u32[]{:S(2)}) copy-start(bf16[2048,256]{1,0:T(8,128)(2,1)} %wq.1) | copy-start | bytes 3145732
  9.0 11.7 %copy-start.2 = (bf16[2048,256]{1,0:T(8,128)(2,1)S(1)}, bf16[2048,256]{1,0:T(8,128)(2,1)}, u32[]{:S(2)}) copy-start(bf16[2048,256]{1,0:T(8,128)(2,1)} %lwq.1) | copy-start | bytes 3145732
  13.2 1.6 %copy-start.12 = (bf16[768,2048]{1,0:T(8,128)(2,1)}, bf16[768,2048]{1,0:T(8,128)(2,1)S(1)}, u32[]{:S(2)}) copy-start(bf16[768,2048]{1,0:T(8,128)(2,1)S(1)} %get-tuple-element.15.normed) | copy-start | bytes 9437188
  14.9 0.7 copy-start.14
  15.6 16.3 %collective-permute-start.2 = (bf16[896,256]{1,0:T(8,128)(2,1)}, bf16[896,256]{1,0:T(8,128)(2,1)S(1)}, u32[]{:S(2)}, u32[]{:S(2)}) collective-permute-start(bf16[896,256]{1,0:T(8,128)(2,1)} %get-tuple-element.18), channel_id=1, source_target_pairs={{8,0},{16,8},{24,16},{0,24},{9,1},{17,9},{25,17},{1,25},{10,2},{18... | collective-permute-start | bytes 1376264 | tf_op jit(solution)/shard_map/ppermute | solution.py:272
  20.7 21.9 %collective-permute-start = (bf16[896,256]{1,0:T(8,128)(2,1)S(1)}, bf16[896,256]{1,0:T(8,128)(2,1)S(1)}, u32[]{:S(2)}, u32[]{:S(2)}) collective-permute-start(bf16[896,256]{1,0:T(8,128)(2,1)S(1)} %get-tuple-element.17.refs_1_), channel_id=1, source_target_pairs={{0,8},{8,16},{16,24},{24,0},{1,9},{9,17},{17,25},{25,1},{2,10},{10... | collective-permute-start | bytes 1376264 | tf_op jit(solution)/shard_map/ppermute | solution.py:271
  20.7 0.9 %copy-start.11 = (f32[3,64,128]{2,1,0:T(8,128)S(1)}, f32[3,64,128]{2,1,0:T(8,128)}, u32[]{:S(2)}) copy-start(f32[3,64,128]{2,1,0:T(8,128)} %constant.90.clone.col_tab) | copy-start | bytes 294916
  21.6 1.9 %copy-start.13 = (bf16[768,2048]{1,0:T(8,128)(2,1)S(1)}, bf16[768,2048]{1,0:T(8,128)(2,1)}, u32[]{:S(2)}) copy-start(bf16[768,2048]{1,0:T(8,128)(2,1)} %copy-done.12) | copy-start | bytes 9437188
  25.6 18.8 %copy-start.9 = (f32[2]{0:T(128)S(1)}, f32[2]{0:T(128)}, u32[]{:S(2)}) copy-start(f32[2]{0:T(128)} %param.25) | copy-start | bytes 28
  25.7 18.8 %copy-start.15 = (bf16[768,256]{1,0:T(8,128)(2,1)S(1)}, bf16[768,256]{1,0:T(8,128)(2,1)}, u32[]{:S(2)}) copy-start(bf16[768,256]{1,0:T(8,128)(2,1)} %copy-done.14) | copy-start | bytes 1179652
  31.9 19.4 %collective-permute-start.3 = (bf16[384,256]{1,0:T(8,128)(2,1)S(1)}, bf16[384,256]{1,0:T(8,128)(2,1)S(1)}, u32[]{:S(2)}, u32[]{:S(2)}) collective-permute-start(bf16[384,256]{1,0:T(8,128)(2,1)S(1)} %slice.25), channel_id=1, source_target_pairs={{8,0},{16,8},{24,16},{0,24},{9,1},{17,9},{25,17},{1,25},{10,2},{18... | collective-permute-start | bytes 589832 | tf_op jit(solution)/shard_map/ppermute | solution.py:296
  42.6 8.7 %collective-permute-start.1 = (bf16[384,256]{1,0:T(8,128)(2,1)S(1)}, bf16[384,256]{1,0:T(8,128)(2,1)S(1)}, u32[]{:S(2)}, u32[]{:S(2)}) collective-permute-start(bf16[384,256]{1,0:T(8,128)(2,1)S(1)} %slice.24), channel_id=1, source_target_pairs={{0,8},{8,16},{16,24},{24,0},{1,9},{9,17},{17,25},{25,1},{2,10},{10... | collective-permute-start | bytes 589832 | tf_op jit(solution)/shard_map/ppermute | solution.py:295
  51.4 3.1 %copy-start.17 = (bf16[256,2048]{1,0:T(8,128)(2,1)S(1)}, bf16[256,2048]{1,0:T(8,128)(2,1)}, u32[]{:S(2)}) copy-start(bf16[256,2048]{1,0:T(8,128)(2,1)} %param.27) | copy-start | bytes 3145732
  51.4 3.1 %copy-start.18 = (bf16[256,2048]{1,0:T(8,128)(2,1)S(1)}, bf16[256,2048]{1,0:T(8,128)(2,1)}, u32[]{:S(2)}) copy-start(bf16[256,2048]{1,0:T(8,128)(2,1)} %param.26) | copy-start | bytes 3145732
  56.3 2.6 %copy-start.16 = (f32[768,2048]{1,0:T(8,128)}, f32[768,2048]{1,0:T(8,128)S(1)}, u32[]{:S(2)}) copy-start(f32[768,2048]{1,0:T(8,128)S(1)} %fusion) | copy-start | bytes 18874372
  59.2 3.5 %collective-permute-start.4 = (bf16[2,2,96,2048]{3,2,1,0:T(8,128)(2,1)S(1)}, bf16[2,2,96,2048]{3,2,1,0:T(8,128)(2,1)S(1)}, u32[]{:S(2)}, u32[]{:S(2)}) collective-permute-start(bf16[2,2,96,2048]{3,2,1,0:T(8,128)(2,1)S(1)} %fusion.4), channel_id=1, source_target_pairs={{0,1},{1,0},{2,3},{3,2},{4,5},{5,4},{6,7},{7,6},{8,9},{9,8},{10,11... | collective-permute-start | bytes 4718600 | tf_op jit(solution)/shard_map/ppermute | solution.py:324
  66.1 11.4 %collective-permute-start.7 = (bf16[2,96,1024]{2,1,0:T(8,128)(2,1)}, bf16[2,96,1024]{2,1,0:T(8,128)(2,1)S(1)}, u32[]{:S(2)}, u32[]{:S(2)}) collective-permute-start(bf16[2,96,1024]{2,1,0:T(8,128)(2,1)} %fusion.9), channel_id=1, source_target_pairs={{0,4},{1,5},{2,6},{3,7},{4,0},{5,1},{6,2},{7,3},{8,12},{9,13},{10,... | collective-permute-start | bytes 1179656 | tf_op jit(solution)/shard_map/ppermute | solution.py:329
  68.4 11.2 %collective-permute-start.5 = (bf16[2,96,1024]{2,1,0:T(8,128)(2,1)}, bf16[2,96,1024]{2,1,0:T(8,128)(2,1)}, u32[]{:S(2)}, u32[]{:S(2)}) collective-permute-start(bf16[2,96,1024]{2,1,0:T(8,128)(2,1)} %fusion.8), channel_id=1, source_target_pairs={{0,2},{1,3},{2,0},{3,1},{4,6},{5,7},{6,4},{7,5},{8,10},{9,11},{10,... | collective-permute-start | bytes 1179656 | tf_op jit(solution)/shard_map/ppermute | solution.py:328
  77.6 6.3 %collective-permute-start.8 = (bf16[96,1024]{1,0:T(8,128)(2,1)S(1)}, bf16[96,1024]{1,0:T(8,128)(2,1)S(1)}, u32[]{:S(2)}, u32[]{:S(2)}) collective-permute-start(bf16[96,1024]{1,0:T(8,128)(2,1)S(1)} %fusion.13), channel_id=1, source_target_pairs={{0,2},{1,3},{2,0},{3,1},{4,6},{5,7},{6,4},{7,5},{8,10},{9,11},{10,... | collective-permute-start | bytes 589832 | tf_op jit(solution)/shard_map/ppermute | solution.py:333
  80.7 5.9 %collective-permute-start.6 = (bf16[96,1024]{1,0:T(8,128)(2,1)S(1)}, bf16[96,1024]{1,0:T(8,128)(2,1)S(1)}, u32[]{:S(2)}, u32[]{:S(2)}) collective-permute-start(bf16[96,1024]{1,0:T(8,128)(2,1)S(1)} %fusion.12), channel_id=1, source_target_pairs={{0,4},{1,5},{2,6},{3,7},{4,0},{5,1},{6,2},{7,3},{8,12},{9,13},{10,... | collective-permute-start | bytes 589832 | tf_op jit(solution)/shard_map/ppermute | solution.py:332
